TPU v7x, 256 devices: a whole 4x4x8 slice. The times are simulated.
256 devices in a mesh: sp: 16 (over y, x), tp: 16 (over z, core).
Axes of the slice: x: 4, y: 4, z: 8, core: 2. Of those that a mesh axis runs over, the one named last changes fastest.
Arguments:
- queries: bfloat16 [16384, 2048], P('sp', 'tp'), may hold values from -8 to 8
- keys: bfloat16 [16384, 1024], P('sp', 'tp'), may hold values from -8 to 8
- values: bfloat16 [16384, 1024], P('sp', 'tp'), may hold values from -6 to 6
- doc_ids: int32 [16384], P('sp'), may hold values from 0 to 7, never falling along the last dimension, each value on 1 to 3072 neighbouring positions
- sink_logits: float32 [32], P('tp'), may hold values from 3 to 6
- out_weight: bfloat16 [2048, 2048], P('tp'), may hold values from -0.75 to 0.75
- residual: bfloat16 [16384, 2048], P(('sp', 'tp')), may hold values from -6 to 6
- norm_gain: float32 [2048], replicated, may hold values from 0.1 to 1.9
- routes: int32 [16384, 2], P(('sp', 'tp')), may hold values from 0 to 15, all different within a row; in each aligned block of 64 rows (0 to 63, 64 to 127, ...) at most 9 rows name the same one
- route_weights: float32 [16384, 2], P(('sp', 'tp')), may hold values from 0.2 to 1
- gate_weight: bfloat16 [16, 2048, 7168], P('sp', None, 'tp'), may hold values from -0.125 to 0.125
- up_weight: bfloat16 [16, 2048, 7168], P('sp', None, 'tp'), may hold values from -0.125 to 0.125
- down_weight: bfloat16 [16, 7168, 2048], P('sp', 'tp'), may hold values from -0.0625 to 0.0625
Outputs:
- layer_output: bfloat16 [16384, 2048], P(('sp', 'tp'))
Inputs may be any that keep to these rules, and one draw needn't show every extreme that they name: `doc_ids`: never falling along the sequence; each document spans 1 to 3072 positions, one exactly that many. `routes`: each row names 2 different experts. In the rows of one device (aligned blocks of 64 rows) no expert is named by more than 9 rows, a bound that some block reaches.
All inputs are finite; a program needn't handle non-finite values.
Results may differ from a plain program's by a relative error of at most 0.015.
Values may be sent and summed in bfloat16 or wider, within the bound.
A program may use at most 128 MiB of HBM per device.

v0:
```python
import math

import jax
import jax.numpy as jnp
from jax import lax
from jax.sharding import PartitionSpec as P

HEAD_DIM = 64
WINDOW = 128


layer_epsilon = 1e-05
masked_score = -1e30


def passed_along(value, axis, steps):
    count = lax.axis_size(axis)
    first, last = (max(0, -steps), min(count, count - steps))
    return lax.ppermute(value, axis, [(source, source + steps) for source in range(first, last)])


def local(
    queries,
    keys,
    values,
    doc_ids,
    sink_logits,
    out_weight,
    residual,
    norm_gain,
    routes,
    route_weights,
    gate_weight,
    up_weight,
    down_weight,
):
    span_rows = queries.shape[0]
    kv_width = keys.shape[1]
    kv_groups = kv_width // HEAD_DIM
    heads_here = queries.shape[1] // HEAD_DIM
    group_ratio = heads_here // kv_groups
    reach_back = WINDOW - 1
    score_scale = 1.0 / math.sqrt(HEAD_DIM)
    doc_float = (doc_ids + 1).astype(jnp.float32)
    key_value = jnp.concatenate([keys, values], axis=1).astype(jnp.float32)
    tail_pairs, tail_docs = (
        passed_along(key_value[span_rows - reach_back :].astype(jnp.bfloat16), "sp", 1).astype(
            jnp.float32
        ),
        passed_along(doc_float[span_rows - reach_back :].astype(jnp.bfloat16), "sp", 1).astype(
            jnp.float32
        ),
    )
    all_keys = jnp.concatenate([tail_pairs[:, :kv_width].astype(jnp.bfloat16), keys], axis=0)
    all_values = jnp.concatenate([tail_pairs[:, kv_width:].astype(jnp.bfloat16), values], axis=0)
    all_docs = jnp.concatenate([tail_docs, doc_float], axis=0)
    block_rows = min(512, span_rows)
    sink_table = sink_logits.reshape(kv_groups, group_ratio, 1)
    offsets = (
        jnp.arange(block_rows)[:, None] + reach_back - jnp.arange(block_rows + reach_back)[None, :]
    )
    window_mask = (offsets >= 0) & (offsets <= reach_back)
    pieces = []
    for block_index in range(span_rows // block_rows):
        first_row = block_index * block_rows
        query_rows = queries[first_row : first_row + block_rows].reshape(
            block_rows, kv_groups, group_ratio, HEAD_DIM
        )
        key_rows = all_keys[first_row : first_row + block_rows + reach_back].reshape(
            block_rows + reach_back, kv_groups, HEAD_DIM
        )
        value_rows = all_values[first_row : first_row + block_rows + reach_back].reshape(
            block_rows + reach_back, kv_groups, HEAD_DIM
        )
        scores = (
            jnp.einsum("bgrd,sgd->grbs", query_rows, key_rows, preferred_element_type=jnp.float32)
            * score_scale
        )
        same_doc = (
            doc_float[first_row : first_row + block_rows][:, None]
            == all_docs[first_row : first_row + block_rows + reach_back][None, :]
        )
        scores = jnp.where(window_mask & same_doc, scores, masked_score)
        row_max = jnp.maximum(scores.max(-1), sink_table)
        exp_scores = jnp.exp(scores - row_max[..., None])
        denominator = exp_scores.sum(-1) + jnp.exp(sink_table - row_max)
        weighted = jnp.einsum(
            "grbs,sgd->bgrd",
            exp_scores.astype(jnp.bfloat16),
            value_rows,
            preferred_element_type=jnp.float32,
        )
        weighted = weighted / jnp.transpose(denominator, (2, 0, 1))[..., None]
        pieces.append(weighted.astype(jnp.bfloat16).reshape(block_rows, heads_here * HEAD_DIM))
    attended = jnp.concatenate(pieces, axis=0)
    token_major = lax.all_to_all(attended, "tp", split_axis=0, concat_axis=1, tiled=True)
    projected = jnp.dot(
        token_major,
        lax.all_gather(out_weight, "tp", axis=0, tiled=True),
        preferred_element_type=jnp.float32,
    )
    stream = residual.astype(jnp.float32) + projected
    mean_value = stream.mean(-1, keepdims=True)
    centred = stream - mean_value
    variance = (centred * centred).mean(-1, keepdims=True)
    normed = (centred * lax.rsqrt(variance + layer_epsilon) * norm_gain).astype(jnp.bfloat16)
    token_count = residual.shape[0]
    width = residual.shape[1]
    route_count = routes.shape[1]
    expert_count = lax.axis_size("sp") * gate_weight.shape[0]
    capacity = 9 * route_count * token_count // (8 * expert_count)
    flat_routes = routes.reshape(-1)
    one_hot = (flat_routes[:, None] == jnp.arange(expert_count)[None, :]).astype(jnp.int32)
    slot_ids = jnp.sum((jnp.cumsum(one_hot, axis=0) - 1) * one_hot, axis=1)
    destination = flat_routes * capacity + slot_ids
    slot_range = jnp.arange(expert_count * capacity)
    selector = jnp.any(
        slot_range[:, None, None] == destination.reshape(token_count, route_count)[None], axis=2
    )
    dispatch = jnp.dot(
        selector.astype(jnp.bfloat16), normed, preferred_element_type=jnp.float32
    ).astype(jnp.bfloat16)
    inbound = lax.all_to_all(
        dispatch.reshape(expert_count, capacity, width),
        "sp",
        split_axis=0,
        concat_axis=0,
        tiled=True,
    )
    arrived = inbound.reshape(-1, width)
    row_piece = lax.all_gather(arrived, "tp", axis=0, tiled=True)
    gate = jnp.dot(row_piece, gate_weight[0], preferred_element_type=jnp.float32)
    upward = jnp.dot(row_piece, up_weight[0], preferred_element_type=jnp.float32)
    hidden = (jax.nn.silu(gate) * upward).astype(jnp.bfloat16)
    partial_value = jnp.dot(hidden, down_weight[0], preferred_element_type=jnp.float32).astype(
        jnp.bfloat16
    )
    returned = lax.psum_scatter(
        lax.optimization_barrier(partial_value).astype(jnp.float32).astype(jnp.bfloat16),
        "tp",
        scatter_dimension=0,
        tiled=True,
    )
    back_rows = lax.all_to_all(
        returned.reshape(inbound.shape), "sp", split_axis=0, concat_axis=0, tiled=True
    ).reshape(-1, width)
    picked = back_rows[destination].astype(jnp.float32).reshape(token_count, route_count, width)
    combined = jnp.sum(picked * route_weights[..., None], axis=1)
    return (stream + combined).astype(jnp.bfloat16)


def solution(mesh):
    placed = (
        P("sp", "tp"),
        P("sp", "tp"),
        P("sp", "tp"),
        P("sp"),
        P("tp"),
        P("tp", None),
        P(("sp", "tp"), None),
        P(),
        P(("sp", "tp"), None),
        P(("sp", "tp"), None),
        P("sp", None, "tp"),
        P("sp", None, "tp"),
        P("sp", "tp", None),
    )
    return jax.shard_map(
        local, mesh=mesh, in_specs=placed, out_specs=P(("sp", "tp"), None), check_vma=False
    )
```

profile of v0, /device:TPU:32, one launch (start us, length us, event | category | flops | bytes accessed | tf_op | source)
XLA Modules:
  0.0 299.0 jit_solution(14459671882906045663)
XLA Ops:
  6.5 0.0 copy-start
  6.5 0.7 all-gather.3.cloned.1.call-update
  7.3 0.7 fusion.76
  8.0 0.1 slice.50
  8.0 3.4 %collective-permute-start.1 = (bf16[127]{0:T(256)(128)(2,1)S(1)}, bf16[127]{0:T(256)(128)(2,1)S(1)}, u32[]{:S(2)}, u32[]{:S(2)}) collective-permute-start(bf16[127]{0:T(256)(128)(2,1)S(1)} %slice.50), channel_id=1, source_target_pairs={{0,16},{16,32},{32,48},{48,64},{64,80},{80,96},{96,112},{112,128},... | collective-permute-start | bytes 770 | tf_op jit(solution)/shard_map/ppermute | solution.py:19
  11.4 0.8 pad_maximum_fusion.3
  12.2 3.4 %collective-permute-start = (bf16[127,128]{0,1:T(8,128)(2,1)S(1)}, bf16[127,128]{0,1:T(8,128)(2,1)S(1)}, u32[]{:S(2)}, u32[]{:S(2)}) collective-permute-start(bf16[127,128]{0,1:T(8,128)(2,1)S(1)} %pad_maximum_fusion.3), channel_id=1, source_target_pairs={{0,16},{16,32},{32,48},{48,64},{64,80},{80,96},{96,112},{112,128},... | collective-permute-start | bytes 97544 | tf_op jit(solution)/shard_map/ppermute | solution.py:19
  15.6 1.0 fusion.78
  16.6 0.1 copy.31
  16.8 0.1 copy.33
  16.9 0.8 copy.38
  17.7 0.1 eq.61
  17.8 0.0 collective-permute-done.1
  17.8 0.1 pad_maximum_fusion.4
  17.9 0.7 compare_and_fusion.1
  18.6 0.0 copy-done.3
  18.6 0.0 copy-start.6
  18.6 0.8 fusion.6
  19.4 0.0 collective-permute-done
  19.4 0.8 fusion.5
  20.2 0.1 broadcast_maximum_fusion.1
  20.3 1.2 fusion.1
  21.5 0.1 fusion.67
  21.6 0.9 fusion.32
  22.5 0.1 copy.35
  22.6 0.0 copy-start.2
  22.6 2.6 fusion.38
  25.3 0.1 copy.36
  25.4 0.7 pad_maximum_fusion
  26.1 8.5 %all-to-all-start = ((bf16[16,64,128]{2,1,0:T(8,128)(2,1)}), bf16[16,64,128]{2,1,0:T(8,128)(2,1)S(1)}, u32[]{:S(2)}, u32[]{:S(2)}) async-start(bf16[16,64,128]{2,1,0:T(8,128)(2,1)} %bitcast.27), calls=%async_computation | async-start | bytes 524288 | tf_op jit(solution)/shard_map/all_to_all | solution.py:96
  34.6 0.0 all-gather.5.cloned.1.call-start
  34.7 0.1 fusion.59
  34.7 0.2 reduce_window_sum.11
  34.9 0.2 select_reduce_fusion
  35.1 0.1 reduce_sum.67
  35.3 0.1 copy.40
  35.3 0.1 fusion.46
  35.4 0.0 copy-start.5
  35.4 10.4 %all-to-all-done = bf16[16,64,128]{2,1,0:T(8,128)(2,1)S(1)} async-done(((bf16[16,64,128]{2,1,0:T(8,128)(2,1)}), bf16[16,64,128]{2,1,0:T(8,128)(2,1)S(1)}, u32[]{:S(2)}, u32[]{:S(2)}) %all-to-all-start) | async-done | bytes 262176 | tf_op jit(solution)/shard_map/all_to_all | solution.py:96
  45.9 25.5 %all-gather.3.cloned.1.call-done = bf16[2048,2048]{1,0:T(8,128)(2,1)} async-done(((bf16[128,2048]{1,0:T(8,128)(2,1)}), bf16[2048,2048]{1,0:T(8,128)(2,1)}) %all-gather.3.cloned.1.call-update) | async-done | bytes 8388624 | tf_op jit(solution)/shard_map/all_gather | solution.py:99
  71.4 5.1 %fusion.81 = (f32[64]{0:T(128)S(1)}, f32[64,2048]{1,0:T(8,128)S(1)}) fusion(bf16[2048,2048]{1,0:T(8,128)(2,1)} %all-gather.3.cloned.1.call-done, bf16[64,2048]{1,0:T(8,128)(2,1)S(1)} %copy-done.2, bf16[16,64,128]{2,1,0:T(8,128)(2,1)S(1)} %all-to-all-done), kind=kOutput, calls=%fused_computation.100 | convolution fusion | flops 537264064 | bytes 9437440 | tf_op jit(solution)/shard_map/dot_general | solution.py:97
  76.5 0.2 multiply_reduce_fusion.1
  76.8 1.2 convolution_convert_fusion.1
  78.0 1.3 reshape.289
  79.3 24.3 %all_to_all.29 = bf16[16,9,2048]{2,1,0:T(8,128)(2,1)} all-to-all(bf16[16,9,2048]{2,1,0:T(8,128)(2,1)S(1)} %reshape.289), channel_id=1, replica_groups=mesh['sp'=16,'tp'=16] {'sp'}, dimensions={0} | all-to-all | bytes 1179648 | tf_op jit(solution)/shard_map/all_to_all | solution.py:123
  103.5 2.3 reshape.290
  105.8 0.0 all-gather.5.cloned.1.call-update
  105.8 0.2 reduce-scatter.2.cloned.1.call-start
  106.1 55.5 %all-gather.5.cloned.1.call-done = bf16[2304,2048]{1,0:T(8,128)(2,1)} async-done(((bf16[144,2048]{1,0:T(8,128)(2,1)}), bf16[2304,2048]{1,0:T(8,128)(2,1)}) %all-gather.5.cloned.1.call-update) | async-done | bytes 9437200 | tf_op jit(solution)/shard_map/all_gather | solution.py:131
  161.6 10.7 %fusion.10 = f32[2304,448]{0,1:T(8,128)} fusion(bf16[2304,2048]{1,0:T(8,128)(2,1)} %all-gather.5.cloned.1.call-done, bf16[1,2048,448]{1,2,0:T(8,128)(2,1)} %param.23), kind=kOutput, calls=%fused_computation.18 | convolution fusion | flops 4227858432 | bytes 15400960 | tf_op jit(solution)/shard_map/dot_general | solution.py:132
  172.2 17.7 %convolution_convert_fusion = bf16[2304,2048]{1,0:T(8,128)(2,1)} fusion(bf16[1,448,2048]{2,1,0:T(8,128)(2,1)S(1)} %copy-done, bf16[2304,2048]{1,0:T(8,128)(2,1)} %all-gather.5.cloned.1.call-done, f32[2304,448]{0,1:T(8,128)} %fusion.10, bf16[1,2048,448]{1,2,0:T(8,128)(2,1)} %param.24), kind=kOutput, calls=%fused_computation.1 | convolution fusion | flops 8466628608 | bytes 26673152 | tf_op jit(solution)/shard_map/dot_general | solution.py:135
  190.0 0.0 reduce-scatter.2.cloned.1.call-update
  190.0 0.0 copy-start.7
  190.0 69.6 %reduce-scatter.2.cloned.1.call-done = bf16[144,2048]{1,0:T(8,128)(2,1)} async-done(((bf16[2304,2048]{1,0:T(8,128)(2,1)}), bf16[144,2048]{1,0:T(8,128)(2,1)}) %reduce-scatter.2.cloned.1.call-update) | async-done | bytes 589840 | tf_op jit(solution)/shard_map/reduce_scatter | solution.py:138
  259.6 2.3 reshape.291
  261.9 6.8 %all-to-all-start.2 = ((bf16[16,9,2048]{2,1,0:T(8,128)(2,1)}), bf16[16,9,2048]{2,1,0:T(8,128)(2,1)}, u32[]{:S(2)}, u32[]{:S(2)}) async-start(bf16[16,9,2048]{2,1,0:T(8,128)(2,1)} %reshape.291), calls=%async_computation.3 | async-start | bytes 2097152 | tf_op jit(solution)/shard_map/all_to_all | solution.py:144
  268.7 0.1 mul.89
  268.9 0.1 copy.41
  269.0 16.3 %all-to-all-done.2 = bf16[16,9,2048]{2,1,0:T(8,128)(2,1)} async-done(((bf16[16,9,2048]{2,1,0:T(8,128)(2,1)}), bf16[16,9,2048]{2,1,0:T(8,128)(2,1)}, u32[]{:S(2)}, u32[]{:S(2)}) %all-to-all-start.2) | async-done | bytes 589856 | tf_op jit(solution)/shard_map/all_to_all | solution.py:144
  285.3 1.5 reshape.292
  286.8 1.7 gather_fusion
  288.5 1.7 reshape.293
  290.2 1.5 multiply_reduce_fusion
  291.7 0.8 add_convert_fusion
  (20 shorter events, 0.1 us)
Async XLA Ops:
  6.5 165.7 %copy-start = (bf16[1,448,2048]{2,1,0:T(8,128)(2,1)S(1)}, bf16[1,448,2048]{2,1,0:T(8,128)(2,1)}, u32[]{:S(2)}) copy-start(bf16[1,448,2048]{2,1,0:T(8,128)(2,1)} %param.25) | copy-start | bytes 5505028
  6.5 12.1 %copy-start.3 = (bf16[1024,64]{0,1:T(8,128)(2,1)S(1)}, bf16[1024,64]{0,1:T(8,128)(2,1)}, u32[]{:S(2)}) copy-start(bf16[1024,64]{0,1:T(8,128)(2,1)} %param.14) | copy-start | bytes 393220
  6.5 64.9 %all-gather.3.cloned.1.call-start = ((), (), s32[]{:S(2)}) async-start(), calls=%async_computation.4 | async-start | bytes 8912896 | tf_op jit(solution)/shard_map/all_gather | solution.py:99
  8.0 9.8 %collective-permute-start.1 = (bf16[127]{0:T(256)(128)(2,1)S(1)}, bf16[127]{0:T(256)(128)(2,1)S(1)}, u32[]{:S(2)}, u32[]{:S(2)}) collective-permute-start(bf16[127]{0:T(256)(128)(2,1)S(1)} %slice.50), channel_id=1, source_target_pairs={{0,16},{16,32},{32,48},{48,64},{64,80},{80,96},{96,112},{112,128},... | collective-permute-start | bytes 770 | tf_op jit(solution)/shard_map/ppermute | solution.py:19
  12.2 7.2 %collective-permute-start = (bf16[127,128]{0,1:T(8,128)(2,1)S(1)}, bf16[127,128]{0,1:T(8,128)(2,1)S(1)}, u32[]{:S(2)}, u32[]{:S(2)}) collective-permute-start(bf16[127,128]{0,1:T(8,128)(2,1)S(1)} %pad_maximum_fusion.3), channel_id=1, source_target_pairs={{0,16},{16,32},{32,48},{48,64},{64,80},{80,96},{96,112},{112,128},... | collective-permute-start | bytes 97544 | tf_op jit(solution)/shard_map/ppermute | solution.py:19
  18.6 1.6 copy-start.6
  19.4 2.1 copy-start.1
  20.3 1.3 copy-start.4
  22.6 48.8 %copy-start.2 = (bf16[64,2048]{1,0:T(8,128)(2,1)S(1)}, bf16[64,2048]{1,0:T(8,128)(2,1)}, u32[]{:S(2)}) copy-start(bf16[64,2048]{1,0:T(8,128)(2,1)} %param.19) | copy-start | bytes 786436
  26.1 19.8 %all-to-all-start = ((bf16[16,64,128]{2,1,0:T(8,128)(2,1)}), bf16[16,64,128]{2,1,0:T(8,128)(2,1)S(1)}, u32[]{:S(2)}, u32[]{:S(2)}) async-start(bf16[16,64,128]{2,1,0:T(8,128)(2,1)} %bitcast.27), calls=%async_computation | async-start | bytes 524288 | tf_op jit(solution)/shard_map/all_to_all | solution.py:96
  34.6 127.0 %all-gather.5.cloned.1.call-start = ((), (), s32[]{:S(2)}) async-start(), calls=%async_computation.5 | async-start | bytes 10027008 | tf_op jit(solution)/shard_map/all_gather | solution.py:131
  35.4 41.3 %copy-start.5 = (f32[2048]{0:T(1024)S(1)}, f32[2048]{0:T(1024)}, u32[]{:S(2)}) copy-start(f32[2048]{0:T(1024)} %param.20) | copy-start | bytes 24580
  105.8 153.8 %reduce-scatter.2.cloned.1.call-start = ((), (), s32[]{:S(2)}) async-start(), calls=%async_computation.6 | async-start | bytes 10027008 | tf_op jit(solution)/shard_map/reduce_scatter | solution.py:138
  190.0 78.9 %copy-start.7 = (f32[64,2]{0,1:T(2,128)S(1)}, f32[64,2]{0,1:T(2,128)}, u32[]{:S(2)}) copy-start(f32[64,2]{0,1:T(2,128)} %param.22) | copy-start | bytes 1540
  261.9 23.4 %all-to-all-start.2 = ((bf16[16,9,2048]{2,1,0:T(8,128)(2,1)}), bf16[16,9,2048]{2,1,0:T(8,128)(2,1)}, u32[]{:S(2)}, u32[]{:S(2)}) async-start(bf16[16,9,2048]{2,1,0:T(8,128)(2,1)} %reshape.291), calls=%async_computation.3 | async-start | bytes 2097152 | tf_op jit(solution)/shard_map/all_to_all | solution.py:144
Sparse Core Ops, SparseCore 0:
  9.2 62.2 all-gather.2
  106.0 55.5 all-gather.4
  190.1 69.4 reduce-scatter.1
where the time goes:
time: 302 us; the launch traced here: 299 us
  waiting for transfers between devices  178 us (59%)
  matrix products  39.7 us (13%)
  blocking collectives  24.3 us (8%)
  starting transfers between devices  22.3 us (7%)
  local copies, waits for them, and re-layouts  13.7 us (5%)
  between operations  13.4 us (4%)
  other arithmetic  7.45 us (2%)
    reduce_scatter x1, waiting for transfers between devices, local(): lax.psum_scatter(lax.optimization_barrier(partial_value).astype(jnp.float...  69.6 us
    all_gather x1, waiting for transfers between devices, local(): row_piece = lax.all_gather(arrived, 'tp', axis=0, tiled=True)  55.5 us
    all_gather x1, waiting for transfers between devices, local(): lax.all_gather(out_weight, 'tp', axis=0, tiled=True)  25.5 us
    all_to_all x1, blocking collectives, local(): lax.all_to_all(dispatch.reshape(expert_count, capacity, width), 'sp', spl...  24.3 us
    dot_general x1, matrix products, local(): jnp.dot(hidden, down_weight[0], preferred_element_type=jnp.float32)  17.7 us
    all_to_all x1, waiting for transfers between devices, local(): lax.all_to_all(returned.reshape(inbound.shape), 'sp', split_axis=0, conca...  16.3 us
    dot_general x1, matrix products, local(): jnp.dot(row_piece, gate_weight[0], preferred_element_type=jnp.float32)  10.7 us
    all_to_all x1, waiting for transfers between devices, local(): lax.all_to_all(attended, 'tp', split_axis=0, concat_axis=1, tiled=True)  10.4 us
  transfers between devices with their start and end apart: 7, of which 5 were waited for; matrix products, arithmetic and copies ran while one was open for 4% of the time, Pallas kernels for 0%

commit v1 on v0

--- a/solution.py
+++ b/solution.py
@@ -1,12 +1,18 @@
+import functools
 import math
 
 import jax
 import jax.numpy as jnp
 from jax import lax
+from jax.experimental import pallas as pl
+from jax.experimental.pallas import tpu as pltpu
 from jax.sharding import PartitionSpec as P
 
 HEAD_DIM = 64
 WINDOW = 128
+ROWS = 144
+HALF = 1024
+MESH = pl.DeviceIdType.MESH
 
 
 layer_epsilon = 1e-05
@@ -17,6 +23,281 @@
     count = lax.axis_size(axis)
     first, last = (max(0, -steps), min(count, count - steps))
     return lax.ppermute(value, axis, [(source, source + steps) for source in range(first, last)])
+
+
+RS_SLOTS = ((3, 1), (4, 0), (2, 1), (3, 0), (1, 1), (2, 0), (1, 0))
+RS_NEEDS = (None, None, 0, 1, 2, 3, 5)
+
+
+def expert_kernel(
+    arrived,
+    gate,
+    up,
+    down,
+    out,
+    rows,
+    partial,
+    partner_partial,
+    sum_up,
+    sum_down,
+    got_up,
+    got_down,
+    gate_v,
+    up_v,
+    down_v,
+    load_sem,
+    ag_send,
+    ag_recv,
+    share_send,
+    share_recv,
+    rs_send,
+    rs_recv,
+    part_send,
+    part_recv,
+):
+    me = lax.axis_index("tp")
+    chip = me // 2
+    core = lax.rem(me, 2)
+    above, below = lax.rem(me + 2, 16), lax.rem(me + 14, 16)
+    partner = me + 1 - 2 * core
+
+    def block(offset):
+        return lax.rem(chip + offset + 8, 8)
+
+    loads = [
+        pltpu.make_async_copy(arrived, rows.at[chip, core], load_sem.at[0]),
+        pltpu.make_async_copy(gate, gate_v, load_sem.at[1]),
+        pltpu.make_async_copy(up, up_v, load_sem.at[2]),
+        pltpu.make_async_copy(down, down_v, load_sem.at[3]),
+    ]
+    for load in loads:
+        load.start()
+
+    barrier = pltpu.get_barrier_semaphore()
+    for other in (above, below, partner):
+        pl.semaphore_signal(barrier, inc=1, device_id={"tp": other}, device_id_type=MESH)
+    pl.semaphore_wait(barrier, 3)
+
+    def piece(origin_offset, half):
+        return rows.at[block(origin_offset), core, :, pl.ds(pl.multiple_of(half * HALF, HALF), HALF)]
+
+    def gather(direction, s, sending):
+        distance = s // 2 + 1
+        travelled = distance - 1 if sending else distance
+        if direction == 0:
+            ref = piece(-travelled, lax.rem(s, 2))
+        else:
+            ref = piece(travelled, 1 - lax.rem(s, 2))
+        return pltpu.make_async_remote_copy(
+            src_ref=ref,
+            dst_ref=ref,
+            send_sem=ag_send.at[direction, s],
+            recv_sem=ag_recv.at[direction, s],
+            device_id={"tp": above if direction == 0 else below},
+            device_id_type=MESH,
+        )
+
+    def share(direction, s, receiving):
+        distance = s // 2 + 1
+        offset = -distance if direction == 0 else distance
+        half = lax.rem(s, 2) if direction == 0 else 1 - lax.rem(s, 2)
+        owner = 1 - core if receiving else core
+        ref = rows.at[block(offset), owner, :, pl.ds(pl.multiple_of(half * HALF, HALF), HALF)]
+        return pltpu.make_async_remote_copy(
+            src_ref=ref,
+            dst_ref=ref,
+            send_sem=share_send.at[direction, s],
+            recv_sem=share_recv.at[direction, s],
+            device_id={"tp": partner},
+            device_id_type=MESH,
+        )
+
+    def share_own(receiving):
+        ref = rows.at[chip, 1 - core if receiving else core]
+        return pltpu.make_async_remote_copy(
+            src_ref=ref,
+            dst_ref=ref,
+            send_sem=share_send.at[0, 7],
+            recv_sem=share_recv.at[0, 7],
+            device_id={"tp": partner},
+            device_id_type=MESH,
+        )
+
+    def share_partial(s, offset):
+        b = block(offset)
+        return pltpu.make_async_remote_copy(
+            src_ref=partial.at[b, 1 - core],
+            dst_ref=partner_partial.at[b],
+            send_sem=part_send.at[s],
+            recv_sem=part_recv.at[s],
+            device_id={"tp": partner},
+            device_id_type=MESH,
+        )
+
+    def reduce_copy(direction, i):
+        source, target = (sum_up, got_up) if direction == 0 else (sum_down, got_down)
+        return pltpu.make_async_remote_copy(
+            src_ref=source.at[i],
+            dst_ref=target.at[i],
+            send_sem=rs_send.at[direction, i],
+            recv_sem=rs_recv.at[direction, i],
+            device_id={"tp": above if direction == 0 else below},
+            device_id_type=MESH,
+        )
+
+    def reduce_step(direction, i):
+        distance, half = RS_SLOTS[i]
+        if direction == 1:
+            distance, half = -distance, 1 - half
+        b = block(distance)
+        need = RS_NEEDS[i]
+        destination, received = (sum_up, got_up) if direction == 0 else (sum_down, got_down)
+        if need is not None:
+            reduce_copy(direction, need).wait_recv()
+
+        def add(r, _):
+            span = pl.ds(pl.multiple_of(r * 16, 16), 16)
+            total = partial[b, core, span, half * HALF : (half + 1) * HALF].astype(jnp.float32)
+            total += partner_partial[b, span, half * HALF : (half + 1) * HALF].astype(jnp.float32)
+            if need is not None:
+                total += received[need, span, :].astype(jnp.float32)
+            destination[i, span, :] = total.astype(jnp.bfloat16)
+            return 0
+
+        lax.fori_loop(0, ROWS // 16, add, 0)
+        reduce_copy(direction, i).start()
+
+    loads[0].wait()
+    for s in (0, 1):
+        for direction in (0, 1):
+            gather(direction, s, True).start()
+    share_own(False).start()
+    for load in loads[1:]:
+        load.wait()
+
+    def offset_of(s):
+        return jnp.where(lax.rem(s, 2) == 0, s // 2, -((s + 1) // 2))
+
+    def step(s, _):
+        @pl.when(s < 7)
+        def _():
+            for direction in (0, 1):
+                gather(direction, s, False).wait_recv()
+
+                @pl.when(s + 2 < 7)
+                def _():
+                    gather(direction, s + 2, True).start()
+
+                share(direction, s, False).start()
+
+        @pl.when(s == 0)
+        def _():
+            share_own(True).wait_recv()
+
+        @pl.when(s < 7)
+        def _():
+            share(0, s, True).wait_recv()
+
+        @pl.when(s > 0)
+        def _():
+            share(1, s - 1, True).wait_recv()
+
+        @pl.when(s == 7)
+        def _():
+            share_partial(6, 3).wait_recv()
+            share_partial(5, -3).wait_recv()
+            reduce_step(0, 0)
+            reduce_step(1, 0)
+
+        b = block(offset_of(s))
+        x = rows[b].reshape(2 * ROWS, 2 * HALF)
+        g = jnp.dot(x, gate_v[...], preferred_element_type=jnp.float32)
+        u = jnp.dot(x, up_v[...], preferred_element_type=jnp.float32)
+        hidden = (g / (1.0 + jnp.exp(-g)) * u).astype(jnp.bfloat16)
+        for n in range(4):
+            y = jnp.dot(hidden, down_v[:, n * 512 : (n + 1) * 512], preferred_element_type=jnp.float32)
+            partial[b, :, :, n * 512 : (n + 1) * 512] = y.astype(jnp.bfloat16).reshape(2, ROWS, 512)
+        share_partial(s, offset_of(s)).start()
+        return 0
+
+    lax.fori_loop(0, 8, step, 0)
+
+    for i in range(1, 7):
+        if i == 1:
+            share_partial(7, -4).wait_recv()
+        if i == 2:
+            share_partial(4, 2).wait_recv()
+            share_partial(3, -2).wait_recv()
+        if i == 4:
+            share_partial(2, 1).wait_recv()
+            share_partial(1, -1).wait_recv()
+        reduce_step(0, i)
+        reduce_step(1, i)
+
+    share_partial(0, 0).wait_recv()
+    for direction in (0, 1):
+        for i in (4, 6):
+            reduce_copy(direction, i).wait_recv()
+    for half, (u_slot, d_slot) in enumerate(((6, 4), (4, 6))):
+        def finish(r, _):
+            span = pl.ds(pl.multiple_of(r * 16, 16), 16)
+            columns = slice(half * HALF, (half + 1) * HALF)
+            total = partial[chip, core, span, columns].astype(jnp.float32)
+            total += partner_partial[chip, span, columns].astype(jnp.float32)
+            total += got_up[u_slot, span, :].astype(jnp.float32)
+            total += got_down[d_slot, span, :].astype(jnp.float32)
+            out[span, columns] = total.astype(jnp.bfloat16)
+            return 0
+
+        lax.fori_loop(0, ROWS // 16, finish, 0)
+
+    share_own(False).wait_send()
+    for s in range(7):
+        for direction in (0, 1):
+            gather(direction, s, True).wait_send()
+            share(direction, s, False).wait_send()
+            reduce_copy(direction, s).wait_send()
+    for s in range(8):
+        share_partial(s, s // 2 if s % 2 == 0 else -((s + 1) // 2)).wait_send()
+
+
+def experts(arrived, gate, up, down):
+    any_space = pl.BlockSpec(memory_space=pltpu.HBM)
+    bf16 = jnp.bfloat16
+    return pl.pallas_call(
+        expert_kernel,
+        out_shape=jax.ShapeDtypeStruct((ROWS, 2 * HALF), bf16),
+        in_specs=[any_space] * 4,
+        out_specs=pl.BlockSpec(memory_space=pltpu.VMEM),
+        scratch_shapes=[
+            pltpu.VMEM((8, 2, ROWS, 2 * HALF), bf16),
+            pltpu.VMEM((8, 2, ROWS, 2 * HALF), bf16),
+            pltpu.VMEM((8, ROWS, 2 * HALF), bf16),
+            pltpu.VMEM((7, ROWS, HALF), bf16),
+            pltpu.VMEM((7, ROWS, HALF), bf16),
+            pltpu.VMEM((7, ROWS, HALF), bf16),
+            pltpu.VMEM((7, ROWS, HALF), bf16),
+            pltpu.VMEM(gate.shape, bf16),
+            pltpu.VMEM(up.shape, bf16),
+            pltpu.VMEM(down.shape, bf16),
+            pltpu.SemaphoreType.DMA((4,)),
+            pltpu.SemaphoreType.DMA((2, 7)),
+            pltpu.SemaphoreType.DMA((2, 7)),
+            pltpu.SemaphoreType.DMA((2, 8)),
+            pltpu.SemaphoreType.DMA((2, 8)),
+            pltpu.SemaphoreType.DMA((2, 7)),
+            pltpu.SemaphoreType.DMA((2, 7)),
+            pltpu.SemaphoreType.DMA((8,)),
+            pltpu.SemaphoreType.DMA((8,)),
+        ],
+        compiler_params=pltpu.CompilerParams(
+            collective_id=1, has_side_effects=True, vmem_limit_bytes=56 * 1024 * 1024
+        ),
+        cost_estimate=pl.CostEstimate(
+            flops=2 * 2304 * 2048 * 448 * 3, bytes_accessed=8 << 20, transcendentals=2304 * 448
+        ),
+        name="experts",
+    )(arrived, gate, up, down)
 
 
 def local(
@@ -128,19 +409,7 @@
         tiled=True,
     )
     arrived = inbound.reshape(-1, width)
-    row_piece = lax.all_gather(arrived, "tp", axis=0, tiled=True)
-    gate = jnp.dot(row_piece, gate_weight[0], preferred_element_type=jnp.float32)
-    upward = jnp.dot(row_piece, up_weight[0], preferred_element_type=jnp.float32)
-    hidden = (jax.nn.silu(gate) * upward).astype(jnp.bfloat16)
-    partial_value = jnp.dot(hidden, down_weight[0], preferred_element_type=jnp.float32).astype(
-        jnp.bfloat16
-    )
-    returned = lax.psum_scatter(
-        lax.optimization_barrier(partial_value).astype(jnp.float32).astype(jnp.bfloat16),
-        "tp",
-        scatter_dimension=0,
-        tiled=True,
-    )
+    returned = experts(arrived, gate_weight[0], up_weight[0], down_weight[0])
     back_rows = lax.all_to_all(
         returned.reshape(inbound.shape), "sp", split_axis=0, concat_axis=0, tiled=True
     ).reshape(-1, width)

time: 302 us -> 243 us (0.80)
  waiting for transfers between devices: 178 us -> 64.9 us
  Pallas kernels: 0 us -> 104 us
  matrix products: 39.7 us -> 9.29 us
  blocking collectives: 24.3 us -> 0 us
  starting transfers between devices: 22.3 us -> 26.3 us
    pallas_call x0 -> x1, Pallas kernels: none -> 104 us  [experts(): pl.pallas_call(expert_kernel, out_shape=jax.ShapeDtypeStruct((ROWS, 2 * H...]
    reduce_scatter x1 -> x0, waiting for transfers between devices: 69.6 us -> none  [local(): lax.psum_scatter(lax.optimization_barrier(partial_value).astype(jnp.float...]
    all_gather x1 -> x0, waiting for transfers between devices: 55.5 us -> none  [local(): row_piece = lax.all_gather(arrived, 'tp', axis=0, tiled=True)]
    dot_general x2 -> x0, matrix products: 28.4 us -> none  [the longest x1 17.7 us: local(): jnp.dot(hidden, down_weight[0], preferred_element_type=jnp.float32)]
    all_to_all x1 -> x0, blocking collectives: 24.3 us -> none  [local(): lax.all_to_all(dispatch.reshape(expert_count, capacity, width), 'sp', spl...]
    all_to_all x0 -> x1, waiting for transfers between devices: none -> 11.6 us  [local(): lax.all_to_all(dispatch.reshape(expert_count, capacity, width), 'sp', spl...]
    all_to_all x0 -> x1, starting transfers between devices: none -> 6.81 us  [local(): lax.all_to_all(dispatch.reshape(expert_count, capacity, width), 'sp', spl...]
    unnamed x18, local copies, waits for them, and re-layouts: 0.91 us -> 7.15 us
  transfers between devices with their start and end apart: 7 -> 6, of which waited for: 5 -> 4; matrix products, arithmetic and copies ran while one was open for 4% -> 8% of each run, Pallas kernels for 0% -> 0%
where the time goes in v1:
time: 243 us; the launch traced here: 242 us
  Pallas kernels  104 us (43%)
  waiting for transfers between devices  64.9 us (27%)
  starting transfers between devices  26.3 us (11%)
  local copies, waits for them, and re-layouts  16.5 us (7%)
  between operations  13.7 us (6%)
  matrix products  9.29 us (4%)
  other arithmetic  7.45 us (3%)
    pallas_call x1, Pallas kernels, experts(): pl.pallas_call(expert_kernel, out_shape=jax.ShapeDtypeStruct((ROWS, 2 * H...  104 us
    all_gather x1, waiting for transfers between devices, local(): lax.all_gather(out_weight, 'tp', axis=0, tiled=True)  25.7 us
    all_to_all x1, waiting for transfers between devices, local(): lax.all_to_all(returned.reshape(inbound.shape), 'sp', split_axis=0, conca...  16.3 us
    all_to_all x1, waiting for transfers between devices, local(): lax.all_to_all(dispatch.reshape(expert_count, capacity, width), 'sp', spl...  11.6 us
    all_to_all x1, waiting for transfers between devices, local(): lax.all_to_all(attended, 'tp', split_axis=0, concat_axis=1, tiled=True)  10.5 us
    all_to_all x1, starting transfers between devices, local(): lax.all_to_all(attended, 'tp', split_axis=0, concat_axis=1, tiled=True)  8.59 us
    unnamed x18, local copies, waits for them, and re-layouts  7.15 us
    all_to_all x1, starting transfers between devices, local(): lax.all_to_all(dispatch.reshape(expert_count, capacity, width), 'sp', spl...  6.81 us
  transfers between devices with their start and end apart: 6, of which 4 were waited for; matrix products, arithmetic and copies ran while one was open for 8% of the time, Pallas kernels for 0%

profile of v1, /device:TPU:32, one launch (start us, length us, event | category | flops | bytes accessed | tf_op | source)
XLA Modules:
  0.0 242.0 jit_solution(6523180711088515465)
XLA Ops:
  6.5 0.0 all-gather.2.cloned.1.call-start
  6.5 0.7 all-gather.2.cloned.1.call-update
  7.3 0.7 fusion.69
  8.0 0.1 slice.50
  8.0 3.4 %collective-permute-start.1 = (bf16[127]{0:T(256)(128)(2,1)S(1)}, bf16[127]{0:T(256)(128)(2,1)S(1)}, u32[]{:S(2)}, u32[]{:S(2)}) collective-permute-start(bf16[127]{0:T(256)(128)(2,1)S(1)} %slice.50), channel_id=1, source_target_pairs={{0,16},{16,32},{32,48},{48,64},{64,80},{80,96},{96,112},{112,128},... | collective-permute-start | bytes 770 | tf_op jit(solution)/shard_map/ppermute | solution.py:25
  11.4 0.8 pad_maximum_fusion.3
  12.2 3.4 %collective-permute-start = (bf16[127,128]{0,1:T(8,128)(2,1)S(1)}, bf16[127,128]{0,1:T(8,128)(2,1)S(1)}, u32[]{:S(2)}, u32[]{:S(2)}) collective-permute-start(bf16[127,128]{0,1:T(8,128)(2,1)S(1)} %pad_maximum_fusion.3), channel_id=1, source_target_pairs={{0,16},{16,32},{32,48},{48,64},{64,80},{80,96},{96,112},{112,128},... | collective-permute-start | bytes 97544 | tf_op jit(solution)/shard_map/ppermute | solution.py:25
  15.6 1.0 fusion.71
  16.6 0.1 copy.35
  16.8 0.1 copy.37
  16.9 0.8 copy.42
  17.7 0.1 eq.61
  17.8 0.0 collective-permute-done.1
  17.8 0.1 pad_maximum_fusion.4
  17.9 0.7 compare_and_fusion.1
  18.6 0.0 copy-done.2
  18.6 0.0 copy-start.5
  18.6 0.8 fusion.5
  19.4 0.0 collective-permute-done
  19.4 0.8 fusion.4
  20.2 0.0 copy-done.5
  20.2 0.1 broadcast_maximum_fusion.1
  20.3 1.2 fusion
  21.5 0.1 fusion.61
  21.6 0.0 copy-done.3
  21.6 0.9 fusion.26
  22.5 0.1 copy.39
  22.6 0.0 copy-start.1
  22.6 1.4 fusion.32
  24.0 1.0 copy.40
  25.1 0.7 pad_maximum_fusion
  25.8 8.6 %all-to-all-start = ((bf16[16,64,128]{2,1,0:T(8,128)(2,1)}), bf16[16,64,128]{2,1,0:T(8,128)(2,1)S(1)}, u32[]{:S(2)}, u32[]{:S(2)}) async-start(bf16[16,64,128]{2,1,0:T(8,128)(2,1)} %bitcast.27), calls=%async_computation | async-start | bytes 524288 | tf_op jit(solution)/shard_map/all_to_all | solution.py:377
  34.4 0.1 fusion.53
  34.5 0.2 reduce_window_sum.11
  34.6 0.2 select_reduce_fusion
  34.8 0.1 reduce_sum.67
  35.0 0.1 copy.44
  35.0 0.1 fusion.40
  35.1 0.0 copy-start.4
  35.2 10.5 %all-to-all-done = bf16[16,64,128]{2,1,0:T(8,128)(2,1)S(1)} async-done(((bf16[16,64,128]{2,1,0:T(8,128)(2,1)}), bf16[16,64,128]{2,1,0:T(8,128)(2,1)S(1)}, u32[]{:S(2)}, u32[]{:S(2)}) %all-to-all-start) | async-done | bytes 262176 | tf_op jit(solution)/shard_map/all_to_all | solution.py:377
  45.7 25.7 %all-gather.2.cloned.1.call-done = bf16[2048,2048]{1,0:T(8,128)(2,1)} async-done(((bf16[128,2048]{1,0:T(8,128)(2,1)}), bf16[2048,2048]{1,0:T(8,128)(2,1)}) %all-gather.2.cloned.1.call-update) | async-done | bytes 8388624 | tf_op jit(solution)/shard_map/all_gather | solution.py:380
  71.4 5.1 %fusion.74 = (f32[64]{0:T(128)S(1)}, f32[64,2048]{1,0:T(8,128)S(1)}) fusion(bf16[2048,2048]{1,0:T(8,128)(2,1)} %all-gather.2.cloned.1.call-done, bf16[64,2048]{1,0:T(8,128)(2,1)S(1)} %copy-done.1, bf16[16,64,128]{2,1,0:T(8,128)(2,1)S(1)} %all-to-all-done), kind=kOutput, calls=%fused_computation.92 | convolution fusion | flops 537264064 | bytes 9437440 | tf_op jit(solution)/shard_map/dot_general | solution.py:378
  76.5 0.0 copy-start
  76.5 0.2 multiply_reduce_fusion.1
  76.8 0.4 convolution_convert_fusion
  77.1 1.2 reshape.289
  78.4 6.8 %all-to-all-start.1 = ((bf16[16,9,2048]{2,1,0:T(8,128)(2,1)}), bf16[16,9,2048]{2,1,0:T(8,128)(2,1)S(1)}, u32[]{:S(2)}, u32[]{:S(2)}) async-start(bf16[16,9,2048]{2,1,0:T(8,128)(2,1)} %reshape.289), calls=%async_computation.1 | async-start | bytes 2097152 | tf_op jit(solution)/shard_map/all_to_all | solution.py:404
  85.2 0.0 copy-done
  85.2 2.4 %copy.45 = bf16[1,2048,448]{2,1,0:T(8,128)(2,1)} copy(bf16[1,2048,448]{1,2,0:T(8,128)(2,1)S(1)} %copy-done) | data formatting | bytes 3670016 | tf_op args[10]
  87.6 3.8 %copy.46 = bf16[1,2048,448]{2,1,0:T(8,128)(2,1)} copy(bf16[1,2048,448]{1,2,0:T(8,128)(2,1)} %param.24) | data formatting | bytes 3670016 | tf_op args[11]
  91.4 11.6 %all-to-all-done.1 = bf16[16,9,2048]{2,1,0:T(8,128)(2,1)S(1)} async-done(((bf16[16,9,2048]{2,1,0:T(8,128)(2,1)}), bf16[16,9,2048]{2,1,0:T(8,128)(2,1)S(1)}, u32[]{:S(2)}, u32[]{:S(2)}) %all-to-all-start.1) | async-done | bytes 589856 | tf_op jit(solution)/shard_map/all_to_all | solution.py:404
  103.0 1.1 reshape.290.arrived
  104.1 103.9 %experts.1 = bf16[144,2048]{1,0:T(8,128)(2,1)} custom-call(bf16[144,2048]{1,0:T(8,128)(2,1)} %reshape.290.arrived, bf16[2048,448]{1,0:T(8,128)(2,1)} %bitcast.150, bf16[2048,448]{1,0:T(8,128)(2,1)} %bitcast.151, bf16[448,2048]{1,0:T(8,128)(2,1)} %bitcast.156), custom_call_target="tpu_custom_call" | custom-call | flops 12683575296 | bytes 8388608 | tf_op jit(solution)/shard_map/experts/pallas_call | solution.py:267
  208.0 0.0 copy-start.6
  208.0 2.3 reshape.291
  210.3 4.1 %all-to-all-start.2 = ((bf16[16,9,2048]{2,1,0:T(8,128)(2,1)}), bf16[16,9,2048]{2,1,0:T(8,128)(2,1)S(1)}, u32[]{:S(2)}, u32[]{:S(2)}) async-start(bf16[16,9,2048]{2,1,0:T(8,128)(2,1)} %reshape.291), calls=%async_computation.2 | async-start | bytes 2097152 | tf_op jit(solution)/shard_map/all_to_all | solution.py:413
  214.4 0.1 mul.80
  214.5 0.1 copy.47
  214.7 16.3 %all-to-all-done.2 = bf16[16,9,2048]{2,1,0:T(8,128)(2,1)S(1)} async-done(((bf16[16,9,2048]{2,1,0:T(8,128)(2,1)}), bf16[16,9,2048]{2,1,0:T(8,128)(2,1)S(1)}, u32[]{:S(2)}, u32[]{:S(2)}) %all-to-all-start.2) | async-done | bytes 589856 | tf_op jit(solution)/shard_map/all_to_all | solution.py:413
  231.0 0.3 reshape.292
  231.2 0.9 gather_fusion
  232.2 0.7 reshape.293
  232.8 1.5 multiply_reduce_fusion
  234.4 0.8 add_convert_fusion
  (14 shorter events, 0.1 us)
Async XLA Ops:
  6.5 12.1 %copy-start.2 = (bf16[1024,64]{0,1:T(8,128)(2,1)S(1)}, bf16[1024,64]{0,1:T(8,128)(2,1)}, u32[]{:S(2)}) copy-start(bf16[1024,64]{0,1:T(8,128)(2,1)} %param.14) | copy-start | bytes 393220
  6.5 64.9 %all-gather.2.cloned.1.call-start = ((), (), s32[]{:S(2)}) async-start(), calls=%async_computation.3 | async-start | bytes 8912896 | tf_op jit(solution)/shard_map/all_gather | solution.py:380
  8.0 9.8 %collective-permute-start.1 = (bf16[127]{0:T(256)(128)(2,1)S(1)}, bf16[127]{0:T(256)(128)(2,1)S(1)}, u32[]{:S(2)}, u32[]{:S(2)}) collective-permute-start(bf16[127]{0:T(256)(128)(2,1)S(1)} %slice.50), channel_id=1, source_target_pairs={{0,16},{16,32},{32,48},{48,64},{64,80},{80,96},{96,112},{112,128},... | collective-permute-start | bytes 770 | tf_op jit(solution)/shard_map/ppermute | solution.py:25
  12.2 7.2 %collective-permute-start = (bf16[127,128]{0,1:T(8,128)(2,1)S(1)}, bf16[127,128]{0,1:T(8,128)(2,1)S(1)}, u32[]{:S(2)}, u32[]{:S(2)}) collective-permute-start(bf16[127,128]{0,1:T(8,128)(2,1)S(1)} %pad_maximum_fusion.3), channel_id=1, source_target_pairs={{0,16},{16,32},{32,48},{48,64},{64,80},{80,96},{96,112},{112,128},... | collective-permute-start | bytes 97544 | tf_op jit(solution)/shard_map/ppermute | solution.py:25
  18.6 1.6 copy-start.5
  20.3 1.3 copy-start.3
  22.6 48.8 %copy-start.1 = (bf16[64,2048]{1,0:T(8,128)(2,1)S(1)}, bf16[64,2048]{1,0:T(8,128)(2,1)}, u32[]{:S(2)}) copy-start(bf16[64,2048]{1,0:T(8,128)(2,1)} %param.19) | copy-start | bytes 786436
  25.8 19.9 %all-to-all-start = ((bf16[16,64,128]{2,1,0:T(8,128)(2,1)}), bf16[16,64,128]{2,1,0:T(8,128)(2,1)S(1)}, u32[]{:S(2)}, u32[]{:S(2)}) async-start(bf16[16,64,128]{2,1,0:T(8,128)(2,1)} %bitcast.27), calls=%async_computation | async-start | bytes 524288 | tf_op jit(solution)/shard_map/all_to_all | solution.py:377
  35.1 41.6 %copy-start.4 = (f32[2048]{0:T(1024)S(1)}, f32[2048]{0:T(1024)}, u32[]{:S(2)}) copy-start(f32[2048]{0:T(1024)} %param.20) | copy-start | bytes 24580
  76.5 8.7 %copy-start = (bf16[1,2048,448]{1,2,0:T(8,128)(2,1)S(1)}, bf16[1,2048,448]{1,2,0:T(8,128)(2,1)}, u32[]{:S(2)}) copy-start(bf16[1,2048,448]{1,2,0:T(8,128)(2,1)} %param.23) | copy-start | bytes 5505028
  78.4 24.7 %all-to-all-start.1 = ((bf16[16,9,2048]{2,1,0:T(8,128)(2,1)}), bf16[16,9,2048]{2,1,0:T(8,128)(2,1)S(1)}, u32[]{:S(2)}, u32[]{:S(2)}) async-start(bf16[16,9,2048]{2,1,0:T(8,128)(2,1)} %reshape.289), calls=%async_computation.1 | async-start | bytes 2097152 | tf_op jit(solution)/shard_map/all_to_all | solution.py:404
  208.0 6.5 %copy-start.6 = (f32[64,2]{0,1:T(2,128)S(1)}, f32[64,2]{0,1:T(2,128)}, u32[]{:S(2)}) copy-start(f32[64,2]{0,1:T(2,128)} %param.22) | copy-start | bytes 1540
  210.3 20.7 %all-to-all-start.2 = ((bf16[16,9,2048]{2,1,0:T(8,128)(2,1)}), bf16[16,9,2048]{2,1,0:T(8,128)(2,1)S(1)}, u32[]{:S(2)}, u32[]{:S(2)}) async-start(bf16[16,9,2048]{2,1,0:T(8,128)(2,1)} %reshape.291), calls=%async_computation.2 | async-start | bytes 2097152 | tf_op jit(solution)/shard_map/all_to_all | solution.py:413
Sparse Core Ops, SparseCore 0:
  9.2 62.2 all-gather.1
